TPU v7x, 32 devices: a whole 2x2x4 slice. The times are simulated.
32 devices in a mesh: kv: 8 (over z, x), tp: 4 (over y, core).
Axes of the slice: x: 2, y: 2, z: 4, core: 2. Of those that a mesh axis runs over, the one named last changes fastest.
Arguments:
- hidden_in: bfloat16 [24, 4096], P('kv'), may hold values from -6 to 6
- norm_gain: float32 [4096], replicated, may hold values from 0.1 to 1.9
- w_query: bfloat16 [4096, 2048], P('kv', 'tp'), may hold values from -0.09375 to 0.09375
- w_key: bfloat16 [4096, 2048], P('kv', 'tp'), may hold values from -0.09375 to 0.09375
- w_value: bfloat16 [4096, 4096], P('kv', 'tp'), may hold values from -0.09375 to 0.09375
- w_out: bfloat16 [4096, 4096], P('kv', 'tp'), may hold values from -0.09375 to 0.09375
- carried_state: float32 [8, 8, 256, 512], P('kv', 'tp'), may hold values from -0.625 to 0.625
- prior_keys: bfloat16 [8, 8, 3, 256], P('kv', 'tp'), may hold values from -0.375 to 0.375
- prior_values: bfloat16 [8, 8, 3, 512], P('kv', 'tp'), may hold values from -6 to 6
- accepted: int32 [8], P('kv'), may hold values from 0 to 3
- lengths: int32 [8], P('kv'), may hold values from 1 to 4096
Outputs:
- layer_out: bfloat16 [24, 4096], P('tp', 'kv')
- committed_state: float32 [8, 8, 256, 512], P('kv', 'tp')
- new_keys: bfloat16 [8, 8, 3, 256], P('kv', 'tp')
- new_values: bfloat16 [8, 8, 3, 512], P('kv', 'tp')
All inputs are finite; a program needn't handle non-finite values.
Results may differ from a plain program's by a relative error of at most 0.014.
Values may be sent and summed in bfloat16 or wider, within the bound.
A program may use at most 64 MiB of HBM per device.

v0:
```python
import jax
import jax.numpy as jnp
from jax import lax
from jax.sharding import PartitionSpec as P

epsilon = 1e-06
rotary_base = 10000.0


def rotate(values, places):
    middle = values.shape[-1] // 2
    inverse = rotary_base ** (-jnp.linspace(0.0, 1.0, middle, dtype=jnp.float32))
    angles = places[..., None] * inverse
    cosine = jnp.cos(angles)[:, :, None, :]
    sine_term = jnp.sin(angles)[:, :, None, :]
    leading = values[..., :middle]
    trailing = values[..., middle:]
    return jnp.concatenate(
        [leading * cosine - trailing * sine_term, leading * sine_term + trailing * cosine], axis=-1
    )


def retain(
    queries,
    key_rows,
    value_rows,
    carried_state,
    prior_keys,
    prior_values,
    accepted,
    lengths,
    head_ids,
):
    steps_ahead = queries.shape[1]
    key_size = queries.shape[-1]
    log_decay = jnp.log(1.0 - 2.0 ** (-5.0 - head_ids))
    slot_ids = jnp.arange(steps_ahead, dtype=jnp.float32)
    places = (lengths + accepted).astype(jnp.float32)[:, None] + slot_ids[None, :]
    turned_q = rotate(queries.astype(jnp.float32), places)
    turned_k = rotate(key_rows.astype(jnp.float32), places) * key_size ** (-0.5)
    taken_count = accepted.astype(jnp.float32)[:, None]
    lag_steps = taken_count[:, :, None] - 1.0 - slot_ids[None, None, :]
    weights_back = jnp.where(
        lag_steps >= 0.0, jnp.exp(log_decay[None, :, None] * jnp.maximum(lag_steps, 0.0)), 0.0
    )
    keep_factor = jnp.exp(log_decay[None, :] * taken_count)
    scaled_keys = prior_keys.astype(jnp.float32) * weights_back[..., None]
    committed = keep_factor[..., None, None] * carried_state + jnp.einsum(
        "shjd,shje->shde",
        scaled_keys,
        prior_values.astype(jnp.float32),
        precision=lax.Precision.HIGHEST,
    )
    reach_decay = jnp.exp(log_decay[None, :] * (slot_ids[:, None] + 1.0))
    carried_part = (
        jnp.einsum("sihd,shde->sihe", turned_q, committed, precision=lax.Precision.HIGHEST)
        * reach_decay[None, :, :, None]
    )
    distance = slot_ids[:, None] - slot_ids[None, :]
    weight = jnp.where(
        distance[None] >= 0.0,
        jnp.exp(log_decay[:, None, None] * jnp.maximum(distance, 0.0)[None]),
        0.0,
    )
    scores = (
        jnp.einsum("sihd,sjhd->shij", turned_q, turned_k, precision=lax.Precision.HIGHEST)
        * weight[None]
    )
    inner_part = jnp.einsum(
        "shij,sjhe->sihe", scores, value_rows.astype(jnp.float32), precision=lax.Precision.HIGHEST
    )
    retained = carried_part + inner_part
    normed = retained * lax.rsqrt(jnp.mean(retained * retained, axis=-1, keepdims=True) + epsilon)
    return (normed.astype(jnp.bfloat16), committed, turned_k)


def body(
    hidden_in,
    norm_gain,
    w_query,
    w_key,
    w_value,
    w_out,
    carried_state,
    prior_keys,
    prior_values,
    accepted,
    lengths,
):
    row_values = hidden_in.astype(jnp.float32)
    normed = (
        row_values
        * lax.rsqrt(jnp.mean(row_values * row_values, axis=-1, keepdims=True) + epsilon)
        * norm_gain
    ).astype(jnp.bfloat16)
    own_rows = normed.shape[0]
    query_width = w_query.shape[1]
    key_width = w_key.shape[1]
    columns = lax.all_to_all(normed, "kv", split_axis=1, concat_axis=0, tiled=True)
    joined = jnp.concatenate((w_query, w_key, w_value), axis=1)
    group_count = lax.axis_size("kv")
    partial_term = jnp.dot(columns, joined, preferred_element_type=jnp.float32)
    grouped = partial_term.reshape(group_count, own_rows, partial_term.shape[1])
    received = lax.all_to_all(grouped, "kv", split_axis=0, concat_axis=0, tiled=True)
    joint_sum = jnp.sum(received, axis=0)
    query_sum = joint_sum[:, :query_width]
    key_sum = joint_sum[:, query_width : query_width + key_width]
    value_sum = joint_sum[:, query_width + key_width :]
    seq_count, head_count, steps_ahead = (
        prior_keys.shape[0],
        prior_keys.shape[1],
        prior_keys.shape[2],
    )

    def by_heads(matrix):
        return matrix.astype(jnp.bfloat16).reshape(seq_count, steps_ahead, head_count, -1)

    value_rows = by_heads(value_sum)
    head_ids = (lax.axis_index("tp") * head_count + jnp.arange(head_count)).astype(jnp.float32)
    heads_out, committed, turned_k = retain(
        by_heads(query_sum),
        by_heads(key_sum),
        value_rows,
        carried_state,
        prior_keys,
        prior_values,
        accepted,
        lengths,
        head_ids,
    )
    flat_rows = heads_out.reshape(own_rows, -1)
    head_terms = lax.dot_general(
        lax.all_gather(flat_rows, "kv", axis=0, tiled=True),
        w_out,
        (((1,), (1,)), ((), ())),
        preferred_element_type=jnp.float32,
    )
    layer_out = lax.psum_scatter(
        head_terms.astype(jnp.bfloat16), "tp", scatter_dimension=0, tiled=True
    )
    new_keys = jnp.transpose(turned_k, (0, 2, 1, 3)).astype(jnp.bfloat16)
    new_values = jnp.transpose(value_rows, (0, 2, 1, 3))
    return (layer_out, committed, new_keys, new_values)


def solution(mesh):
    in_specs = (
        P("kv", None),
        P(),
        P("kv", "tp"),
        P("kv", "tp"),
        P("kv", "tp"),
        P("kv", "tp"),
        P("kv", "tp", None, None),
        P("kv", "tp", None, None),
        P("kv", "tp", None, None),
        P("kv"),
        P("kv"),
    )
    out_specs = (
        P("tp", "kv"),
        P("kv", "tp", None, None),
        P("kv", "tp", None, None),
        P("kv", "tp", None, None),
    )
    return jax.shard_map(body, mesh=mesh, in_specs=in_specs, out_specs=out_specs, check_vma=False)
```

profile of v0, /device:TPU:1, one launch (start us, length us, event | category | flops | bytes accessed | tf_op | source)
XLA Modules:
  0.0 75.8 jit_solution(14520870958238705790)
XLA Ops:
  0.6 0.0 copy-start
  0.6 1.0 %fusion.6 = f32[3]{0:T(128)S(1)} fusion(bf16[3,4096]{1,0:T(4,128)(2,1)} %param.13), kind=kLoop, calls=%fused_computation.13 | loop fusion | flops 36861 | bytes 24588 | tf_op jit(solution)/shard_map/reduce_sum | solution.py:93
  1.6 1.5 %fusion.8 = bf16[3,4096]{1,0:T(4,128)(2,1)} fusion(bf16[3,4096]{1,0:T(4,128)(2,1)} %param.13, f32[4096]{0:T(1024)} %param.14, f32[3]{0:T(128)S(1)} %add_rsqrt_fusion.1), kind=kLoop, calls=%fused_computation.15 | loop fusion | flops 49152 | bytes 65548 | tf_op jit(solution)/shard_map/convert_element_type | solution.py:95
  3.1 6.3 %all-to-all-start = ((bf16[3,8,512]{2,0,1:T(4,128)(2,1)}), bf16[3,8,512]{2,0,1:T(4,128)(2,1)S(1)}, u32[]{:S(2)}, u32[]{:S(2)}) async-start(bf16[3,8,512]{2,0,1:T(4,128)(2,1)} %bitcast.6), calls=%async_computation | async-start | bytes 65536 | tf_op jit(solution)/shard_map/all_to_all | solution.py:99
  10.9 0.1 multiply_exponential_fusion
  10.9 0.1 fusion.20
  11.0 0.1 exponential_select_fusion
  11.1 0.1 multiply_cosine_fusion
  11.2 0.8 %multiply_bitcast_fusion = f32[2,3,256]{2,0,1:T(2,128)S(1)} fusion(bf16[1,2,3,256]{3,1,2,0:T(2,128)(2,1)} %param.20, f32[2,3]{0,1:T(4,128)S(1)} %exponential_select_fusion), kind=kLoop, calls=%fused_computation.28 | loop fusion | flops 3072 | bytes 9240 | tf_op jit(solution)/shard_map/reshape.14
  12.0 1.2 %dynamic-slice.4 = u32[1]{0:T(128)} dynamic-slice(u32[32]{0:T(128)} %constant.49, u32[]{:S(6)} %partition-id.5), dynamic_slice_sizes={1} | dynamic-slice | bytes 12
  13.9 0.0 copy-start.3
  13.9 1.1 %all-to-all-done = bf16[3,8,512]{2,0,1:T(4,128)(2,1)S(1)} async-done(((bf16[3,8,512]{2,0,1:T(4,128)(2,1)}), bf16[3,8,512]{2,0,1:T(4,128)(2,1)S(1)}, u32[]{:S(2)}, u32[]{:S(2)}) %all-to-all-start) | async-done | bytes 24608 | tf_op jit(solution)/shard_map/all_to_all | solution.py:99
  15.0 2.0 %fusion.1 = f32[8,3,2048]{2,0,1:T(8,128)S(1)} fusion(bf16[512,1024]{1,0:T(8,128)(2,1)} %param.17, bf16[512,512]{1,0:T(8,128)(2,1)} %param.16, bf16[512,512]{1,0:T(8,128)(2,1)} %param.15, bf16[3,8,512]{2,0,1:T(4,128)(2,1)S(1)} %all-to-all-done), kind=kOutput, calls=%fused_computation.1 | convolution fusion | flops 56623104 | bytes 2318336 | tf_op jit(solution)/shard_map/dot_general | solution.py:102
  17.0 0.8 %copy.24 = f32[8,3,2048]{2,1,0:T(4,128)} copy(f32[8,3,2048]{2,0,1:T(8,128)S(1)} %fusion.1) | data formatting | bytes 393216 | tf_op jit(solution)/shard_map/dot_general | solution.py:102
  17.8 4.4 %all-to-all-start.1 = ((f32[8,3,2048]{2,1,0:T(4,128)}), f32[8,3,2048]{2,1,0:T(4,128)S(1)}, u32[]{:S(2)}, u32[]{:S(2)}) async-start(f32[8,3,2048]{2,1,0:T(4,128)} %copy.24), calls=%async_computation.1 | async-start | bytes 524288 | tf_op jit(solution)/shard_map/all_to_all | solution.py:104
  22.2 0.7 fusion.2
  22.9 0.0 copy-start.1
  22.9 6.4 %all-to-all-done.1 = f32[8,3,2048]{2,1,0:T(4,128)S(1)} async-done(((f32[8,3,2048]{2,1,0:T(4,128)}), f32[8,3,2048]{2,1,0:T(4,128)S(1)}, u32[]{:S(2)}, u32[]{:S(2)}) %all-to-all-start.1) | async-done | bytes 196640 | tf_op jit(solution)/shard_map/all_to_all | solution.py:104
  29.4 0.1 reduce_sum.28
  29.5 0.1 convolution_multiply_fusion
  29.6 0.1 convolution_bitcast_fusion.1
  29.7 0.7 multiply_reduce_fusion
  30.5 0.1 multiply_convert_fusion
  30.6 24.5 %all-gather = bf16[8,3,1024]{2,1,0:T(4,128)(2,1)S(1)} all-gather(bf16[1,3,1024]{2,1,0:T(4,128)(2,1)S(1)} %bitcast.60), channel_id=1, replica_groups=mesh['kv'=8,'tp'=4] {'kv'}, dimensions={0}, use_global_device_ids=true | all-gather | bytes 55296 | tf_op jit(solution)/shard_map/all_gather | solution.py:133
  55.1 0.4 convolution_convert_fusion
  55.5 14.2 %fusion = bf16[8,512]{1,0:T(8,128)(2,1)S(1)} fusion(bf16[24,512]{1,0:T(8,128)(2,1)S(1)} %convolution_convert_fusion), kind=kCustom, calls=%all-reduce-scatter | all-reduce-scatter fusion | flops 16385 | bytes 33280
  69.7 4.2 %collective-permute-start = (bf16[6,512]{1,0:T(8,128)(2,1)S(1)}, bf16[6,512]{1,0:T(8,128)(2,1)S(1)}, u32[]{:S(2)}, u32[]{:S(2)}) collective-permute-start(bf16[6,512]{1,0:T(8,128)(2,1)S(1)} %slice.38), channel_id=1, source_target_pairs={{0,1},{1,2},{2,3},{4,5},{5,6},{6,7},{8,9},{9,10},{10,11},{12,13},{... | collective-permute-start | bytes 18440
  73.9 0.6 reshape.407
  74.5 0.6 copy.25
  75.1 0.0 collective-permute-done
  75.1 0.1 concatenate.34
  75.2 0.6 constant_dynamic-slice_fusion
  (24 shorter events, 0.2 us)
Async XLA Ops:
  0.6 54.5 %copy-start = (bf16[512,1024]{1,0:T(8,128)(2,1)S(1)}, bf16[512,1024]{1,0:T(8,128)(2,1)}, u32[]{:S(2)}) copy-start(bf16[512,1024]{1,0:T(8,128)(2,1)} %param.18) | copy-start | bytes 3145732
  3.1 11.9 %all-to-all-start = ((bf16[3,8,512]{2,0,1:T(4,128)(2,1)}), bf16[3,8,512]{2,0,1:T(4,128)(2,1)S(1)}, u32[]{:S(2)}, u32[]{:S(2)}) async-start(bf16[3,8,512]{2,0,1:T(4,128)(2,1)} %bitcast.6), calls=%async_computation | async-start | bytes 65536 | tf_op jit(solution)/shard_map/all_to_all | solution.py:99
  13.9 8.3 %copy-start.3 = (bf16[1,2,3,512]{3,1,2,0:T(2,128)(2,1)S(1)}, bf16[1,2,3,512]{3,1,2,0:T(2,128)(2,1)}, u32[]{:S(2)}) copy-start(bf16[1,2,3,512]{3,1,2,0:T(2,128)(2,1)} %param.21) | copy-start | bytes 18436
  15.0 7.2 %copy-start.2 = (f32[1,2,256,512]{3,2,1,0:T(8,128)S(1)}, f32[1,2,256,512]{3,2,1,0:T(8,128)}, u32[]{:S(2)}) copy-start(f32[1,2,256,512]{3,2,1,0:T(8,128)} %param.19) | copy-start | bytes 3145732
  17.8 11.5 %all-to-all-start.1 = ((f32[8,3,2048]{2,1,0:T(4,128)}), f32[8,3,2048]{2,1,0:T(4,128)S(1)}, u32[]{:S(2)}, u32[]{:S(2)}) async-start(f32[8,3,2048]{2,1,0:T(4,128)} %copy.24), calls=%async_computation.1 | async-start | bytes 524288 | tf_op jit(solution)/shard_map/all_to_all | solution.py:104
  22.9 32.6 %copy-start.1 = (f32[1,2,256,512]{3,2,1,0:T(8,128)}, f32[1,2,256,512]{3,2,1,0:T(8,128)S(1)}, u32[]{:S(2)}) copy-start(f32[1,2,256,512]{3,2,1,0:T(8,128)S(1)} %fusion.2) | copy-start | bytes 3145732
  69.7 5.4 %collective-permute-start = (bf16[6,512]{1,0:T(8,128)(2,1)S(1)}, bf16[6,512]{1,0:T(8,128)(2,1)S(1)}, u32[]{:S(2)}, u32[]{:S(2)}) collective-permute-start(bf16[6,512]{1,0:T(8,128)(2,1)S(1)} %slice.38), channel_id=1, source_target_pairs={{0,1},{1,2},{2,3},{4,5},{5,6},{6,7},{8,9},{9,10},{10,11},{12,13},{... | collective-permute-start | bytes 18440
where the time goes:
time: 76.3 us; the launch traced here: 75.8 us
  blocking collectives  38.7 us (51%)
  starting transfers between devices  14.9 us (20%)
  waiting for transfers between devices  7.55 us (10%)
  matrix products  4.06 us (5%)
  local copies, waits for them, and re-layouts  4.05 us (5%)
  other arithmetic  3.82 us (5%)
  between operations  2.77 us (4%)
    all_gather x1, blocking collectives, body(): lax.all_gather(flat_rows, 'kv', axis=0, tiled=True)  24.5 us
    unnamed x1, blocking collectives  14.2 us
    all_to_all x1, waiting for transfers between devices, body(): lax.all_to_all(grouped, 'kv', split_axis=0, concat_axis=0, tiled=True)  6.45 us
    all_to_all x1, starting transfers between devices, body(): lax.all_to_all(normed, 'kv', split_axis=1, concat_axis=0, tiled=True)  6.34 us
    all_to_all x1, starting transfers between devices, body(): lax.all_to_all(grouped, 'kv', split_axis=0, concat_axis=0, tiled=True)  4.36 us
    unnamed x1, starting transfers between devices  4.18 us
    unnamed x14, local copies, waits for them, and re-layouts  2.59 us
    dot_general x1, matrix products, body(): partial_term = jnp.dot(columns, joined, preferred_element_type=jnp.float32)  1.98 us
  transfers between devices with their start and end apart: 3, of which 2 were waited for; matrix products, arithmetic and copies ran while one was open for 6% of the time, Pallas kernels for 0%

commit v1 on v0

--- a/solution.py
+++ b/solution.py
@@ -96,7 +96,12 @@
     own_rows = normed.shape[0]
     query_width = w_query.shape[1]
     key_width = w_key.shape[1]
-    columns = lax.all_to_all(normed, "kv", split_axis=1, concat_axis=0, tiled=True)
+    columns = jnp.concatenate(
+        jax.lax.all_to_all(
+            jnp.stack(jnp.split(normed, jax.lax.axis_size("kv"), 1), axis=0), "kv", 0, 0
+        ),
+        0,
+    )
     joined = jnp.concatenate((w_query, w_key, w_value), axis=1)
     group_count = lax.axis_size("kv")
     partial_term = jnp.dot(columns, joined, preferred_element_type=jnp.float32)

time: 76.3 us -> 80.4 us (1.054)
  local copies, waits for them, and re-layouts: 4.05 us -> 8.82 us
    unnamed x14 -> x21, local copies, waits for them, and re-layouts: 2.59 us -> 6.76 us
  transfers between devices with their start and end apart: 3 -> 3, of which waited for: 2 -> 2; matrix products, arithmetic and copies ran while one was open for 6% -> 5% of each run, Pallas kernels for 0% -> 0%
where the time goes in v1:
time: 80.4 us; the launch traced here: 80 us
  blocking collectives  38.7 us (48%)
  starting transfers between devices  14.9 us (19%)
  local copies, waits for them, and re-layouts  8.82 us (11%)
  waiting for transfers between devices  7.55 us (9%)
  matrix products  4.06 us (5%)
  other arithmetic  3.21 us (4%)
  between operations  2.78 us (3%)
    all_gather x1, blocking collectives, body(): lax.all_gather(flat_rows, 'kv', axis=0, tiled=True)  24.5 us
    unnamed x1, blocking collectives  14.2 us
    unnamed x21, local copies, waits for them, and re-layouts  6.76 us
    all_to_all x1, waiting for transfers between devices, body(): lax.all_to_all(grouped, 'kv', split_axis=0, concat_axis=0, tiled=True)  6.45 us
    all_to_all x1, starting transfers between devices, body(): jax.lax.all_to_all(jnp.stack(jnp.split(normed, jax.lax.axis_size('kv'), 1...  6.34 us
    all_to_all x1, starting transfers between devices, body(): lax.all_to_all(grouped, 'kv', split_axis=0, concat_axis=0, tiled=True)  4.36 us
    unnamed x1, starting transfers between devices  4.18 us
    dot_general x1, matrix products, body(): partial_term = jnp.dot(columns, joined, preferred_element_type=jnp.float32)  1.98 us
  transfers between devices with their start and end apart: 3, of which 2 were waited for; matrix products, arithmetic and copies ran while one was open for 5% of the time, Pallas kernels for 0%

profile of v1, /device:TPU:1, one launch (start us, length us, event | category | flops | bytes accessed | tf_op | source)
XLA Modules:
  0.0 80.0 jit_solution(15221966568025053566)
XLA Ops:
  0.6 1.0 %fusion.6 = f32[3]{0:T(128)S(1)} fusion(bf16[3,4096]{1,0:T(4,128)(2,1)} %param.13), kind=kLoop, calls=%fused_computation.13 | loop fusion | flops 36861 | bytes 24588 | tf_op jit(solution)/shard_map/reduce_sum | solution.py:93
  1.6 0.9 %fusion.8 = bf16[3,4096]{1,0:T(4,128)(2,1)S(1)} fusion(bf16[3,4096]{1,0:T(4,128)(2,1)} %param.13, f32[4096]{0:T(1024)} %param.14, f32[3]{0:T(128)S(1)} %add_rsqrt_fusion.1), kind=kLoop, calls=%fused_computation.15 | loop fusion | flops 49152 | bytes 65548 | tf_op jit(solution)/shard_map/convert_element_type | solution.py:95
  2.5 0.6 constant_dynamic-update-slice_fusion.7
  3.1 0.6 constant_dynamic-update-slice_fusion.6
  3.7 0.6 constant_dynamic-update-slice_fusion.5
  4.3 0.6 constant_dynamic-update-slice_fusion.4
  4.9 0.6 constant_dynamic-update-slice_fusion.3
  5.5 0.6 constant_dynamic-update-slice_fusion.2
  6.1 0.6 constant_dynamic-update-slice_fusion.1
  6.7 0.6 constant_dynamic-update-slice_fusion
  7.3 6.3 %all-to-all-start = ((bf16[8,3,512]{2,1,0:T(4,128)(2,1)}), bf16[8,3,512]{2,1,0:T(4,128)(2,1)S(1)}, u32[]{:S(2)}, u32[]{:S(2)}) async-start(bf16[8,3,512]{2,1,0:T(4,128)(2,1)} %constant_dynamic-update-slice_fusion), calls=%async_computation | async-start | bytes 65536 | tf_op jit(solution)/shard_map/all_to_all | solution.py:100
  15.1 0.1 fusion.19
  15.3 0.1 multiply_cosine_fusion
  15.4 0.8 multiply_bitcast_fusion
  16.1 1.2 %dynamic-slice.4 = u32[1]{0:T(128)} dynamic-slice(u32[32]{0:T(128)} %constant.49, u32[]{:S(6)} %partition-id.5), dynamic_slice_sizes={1} | dynamic-slice | bytes 12
  18.1 1.1 %all-to-all-done = bf16[8,3,512]{2,1,0:T(4,128)(2,1)S(1)} async-done(((bf16[8,3,512]{2,1,0:T(4,128)(2,1)}), bf16[8,3,512]{2,1,0:T(4,128)(2,1)S(1)}, u32[]{:S(2)}, u32[]{:S(2)}) %all-to-all-start) | async-done | bytes 24608 | tf_op jit(solution)/shard_map/all_to_all | solution.py:100
  19.2 2.0 %fusion.1 = f32[8,3,2048]{2,0,1:T(8,128)S(1)} fusion(bf16[512,1024]{1,0:T(8,128)(2,1)} %param.17, bf16[512,512]{1,0:T(8,128)(2,1)} %param.16, bf16[512,512]{1,0:T(8,128)(2,1)} %param.15, bf16[8,3,512]{2,1,0:T(4,128)(2,1)S(1)} %all-to-all-done), kind=kOutput, calls=%fused_computation.1 | convolution fusion | flops 56623104 | bytes 2318336 | tf_op jit(solution)/shard_map/dot_general | solution.py:107
  21.1 0.8 %copy.109 = f32[8,3,2048]{2,1,0:T(4,128)} copy(f32[8,3,2048]{2,0,1:T(8,128)S(1)} %fusion.1) | data formatting | bytes 393216 | tf_op jit(solution)/shard_map/dot_general | solution.py:107
  22.0 4.4 %all-to-all-start.1 = ((f32[8,3,2048]{2,1,0:T(4,128)}), f32[8,3,2048]{2,1,0:T(4,128)S(1)}, u32[]{:S(2)}, u32[]{:S(2)}) async-start(f32[8,3,2048]{2,1,0:T(4,128)} %copy.109), calls=%async_computation.1 | async-start | bytes 524288 | tf_op jit(solution)/shard_map/all_to_all | solution.py:109
  26.4 0.7 fusion.2
  27.1 6.4 %all-to-all-done.1 = f32[8,3,2048]{2,1,0:T(4,128)S(1)} async-done(((f32[8,3,2048]{2,1,0:T(4,128)}), f32[8,3,2048]{2,1,0:T(4,128)S(1)}, u32[]{:S(2)}, u32[]{:S(2)}) %all-to-all-start.1) | async-done | bytes 196640 | tf_op jit(solution)/shard_map/all_to_all | solution.py:109
  33.6 0.1 convolution_multiply_fusion
  33.8 0.1 convolution_bitcast_fusion.1
  33.9 0.7 multiply_reduce_fusion
  34.7 0.1 multiply_convert_fusion
  34.7 24.5 %all-gather = bf16[8,3,1024]{2,1,0:T(4,128)(2,1)S(1)} all-gather(bf16[1,3,1024]{2,1,0:T(4,128)(2,1)S(1)} %bitcast.88), channel_id=1, replica_groups=mesh['kv'=8,'tp'=4] {'kv'}, dimensions={0}, use_global_device_ids=true | all-gather | bytes 55296 | tf_op jit(solution)/shard_map/all_gather | solution.py:138
  59.3 0.4 convolution_convert_fusion
  59.7 14.2 %fusion = bf16[8,512]{1,0:T(8,128)(2,1)S(1)} fusion(bf16[24,512]{1,0:T(8,128)(2,1)S(1)} %convolution_convert_fusion), kind=kCustom, calls=%all-reduce-scatter | all-reduce-scatter fusion | flops 16385 | bytes 33280
  73.9 4.2 %collective-permute-start = (bf16[6,512]{1,0:T(8,128)(2,1)S(1)}, bf16[6,512]{1,0:T(8,128)(2,1)S(1)}, u32[]{:S(2)}, u32[]{:S(2)}) collective-permute-start(bf16[6,512]{1,0:T(8,128)(2,1)S(1)} %slice.38), channel_id=1, source_target_pairs={{0,1},{1,2},{2,3},{4,5},{5,6},{6,7},{8,9},{9,10},{10,11},{12,13},{... | collective-permute-start | bytes 18440
  78.1 0.6 reshape.405
  78.7 0.6 copy.110
  79.3 0.6 constant_dynamic-slice_fusion
  (32 shorter events, 0.5 us)
Async XLA Ops:
  0.6 58.6 %copy-start = (bf16[512,1024]{1,0:T(8,128)(2,1)S(1)}, bf16[512,1024]{1,0:T(8,128)(2,1)}, u32[]{:S(2)}) copy-start(bf16[512,1024]{1,0:T(8,128)(2,1)} %param.18) | copy-start | bytes 3145732
  7.3 11.9 %all-to-all-start = ((bf16[8,3,512]{2,1,0:T(4,128)(2,1)}), bf16[8,3,512]{2,1,0:T(4,128)(2,1)S(1)}, u32[]{:S(2)}, u32[]{:S(2)}) async-start(bf16[8,3,512]{2,1,0:T(4,128)(2,1)} %constant_dynamic-update-slice_fusion), calls=%async_computation | async-start | bytes 65536 | tf_op jit(solution)/shard_map/all_to_all | solution.py:100
  18.0 8.3 %copy-start.3 = (bf16[1,2,3,512]{3,1,2,0:T(2,128)(2,1)S(1)}, bf16[1,2,3,512]{3,1,2,0:T(2,128)(2,1)}, u32[]{:S(2)}) copy-start(bf16[1,2,3,512]{3,1,2,0:T(2,128)(2,1)} %param.21) | copy-start | bytes 18436
  19.2 7.2 %copy-start.2 = (f32[1,2,256,512]{3,2,1,0:T(8,128)S(1)}, f32[1,2,256,512]{3,2,1,0:T(8,128)}, u32[]{:S(2)}) copy-start(f32[1,2,256,512]{3,2,1,0:T(8,128)} %param.19) | copy-start | bytes 3145732
  22.0 11.5 %all-to-all-start.1 = ((f32[8,3,2048]{2,1,0:T(4,128)}), f32[8,3,2048]{2,1,0:T(4,128)S(1)}, u32[]{:S(2)}, u32[]{:S(2)}) async-start(f32[8,3,2048]{2,1,0:T(4,128)} %copy.109), calls=%async_computation.1 | async-start | bytes 524288 | tf_op jit(solution)/shard_map/all_to_all | solution.py:109
  27.1 32.6 %copy-start.1 = (f32[1,2,256,512]{3,2,1,0:T(8,128)}, f32[1,2,256,512]{3,2,1,0:T(8,128)S(1)}, u32[]{:S(2)}) copy-start(f32[1,2,256,512]{3,2,1,0:T(8,128)S(1)} %fusion.2) | copy-start | bytes 3145732
  73.9 5.4 %collective-permute-start = (bf16[6,512]{1,0:T(8,128)(2,1)S(1)}, bf16[6,512]{1,0:T(8,128)(2,1)S(1)}, u32[]{:S(2)}, u32[]{:S(2)}) collective-permute-start(bf16[6,512]{1,0:T(8,128)(2,1)S(1)} %slice.38), channel_id=1, source_target_pairs={{0,1},{1,2},{2,3},{4,5},{5,6},{6,7},{8,9},{9,10},{10,11},{12,13},{... | collective-permute-start | bytes 18440
